TPU v7x, 512 devices: a whole 4x4x16 slice. The times are simulated.
512 devices in a mesh: sp: 16 (over y, x), tp: 32 (over z, core).
Axes of the slice: x: 4, y: 4, z: 16, core: 2. Of those that a mesh axis runs over, the one named last changes fastest.
Arguments:
- tokens: bfloat16 [32, 2048, 4096], P('tp', 'sp'), may hold values from -6 to 6
- latent_down_matrix: bfloat16 [4096, 512], P('tp'), may hold values from -0.09375 to 0.09375
- rope_weight: bfloat16 [4096, 64], P('tp'), may hold values from -0.09375 to 0.09375
- latent_norm_scale: float32 [512], replicated, may hold values from 0.1 to 1.9
- key_up_matrix: bfloat16 [512, 32, 128], P(None, 'tp'), may hold values from -0.25 to 0.25
- value_up_matrix: bfloat16 [512, 32, 128], P(None, 'tp'), may hold values from -0.25 to 0.25
- query: bfloat16 [32, 32, 192], P('sp', 'tp'), may hold values from -126 to 126
Outputs:
- plain_key_cache: bfloat16 [32, 2048, 32, 128], P('sp', None, 'tp')
- head_value_cache: bfloat16 [32, 2048, 32, 128], P('sp', None, 'tp')
- rotated_key_cache: bfloat16 [32, 2048, 64], P('sp')
- first_read: bfloat16 [32, 32, 128], P('sp', 'tp')
All inputs are finite; a program needn't handle non-finite values.
Results may differ from a plain program's by a relative error of at most 0.035.
Values may be sent and summed in bfloat16 or wider, within the bound.
A program may use at most 64 MiB of HBM per device.

v0:
```python
import functools

import numpy as np
import jax
import jax.numpy as jnp
from jax import lax
from jax.sharding import PartitionSpec as P
from jax.experimental import pallas as pl
from jax.experimental.pallas import tpu as pltpu

CORES = 2
PARTS = 4
BF16 = jnp.bfloat16
F32 = jnp.float32


def turn_tables(positions, width):
    half = width // 2
    freqs = (1.0 / np.float32(10000.0) ** (np.arange(half, dtype=np.float32) * np.float32(2.0) / np.float32(width))).astype(np.float32)
    angles = positions.astype(np.float32)[:, None] * freqs
    cosine = np.cos(angles).astype(np.float32)
    sine = np.sin(angles).astype(np.float32)
    return np.concatenate([cosine, cosine], -1), np.concatenate([-sine, sine], -1)


def turn(part, cosine, sine):
    half = part.shape[-1] // 2
    swapped = jnp.concatenate([part[:, half:], part[:, :half]], axis=-1)
    return part * cosine + swapped * sine


def move_kernel(planes, spots, tok, wl, wr, scale, cos_hbm, sin_hbm, kup, vup, x_out, rot_out, up_out,
                tokens, wlat, wrope, acc, acct, other, othert, spread, spreadt, kbuf, vbuf, upbuf, cos_ref, sin_ref,
                tok_s, tok_r, own_s, z_s, z_r, zo_s, x_s, x_r, y_s, y_r, dx_s, dx_r, dy_s, dy_r,
                acc_s, acc_r, g_s, g_r, f_s, f_r, p_s, p_r, up_s):
    s = lax.axis_index("sp")
    t = lax.axis_index("tp")
    z = t // CORES
    c = t % CORES
    rows, lat = wl.shape
    rope = wr.shape[0]
    span = tok.shape[1]
    quarter = rows // 4
    eighth = quarter // 2
    rpart = rope // 4
    half = span // PARTS
    q = s % 4
    sx = s + 1 - 2 * (s % 2)
    sy = s + 2 - 4 * ((s // 2) % 2)
    qx = q + 1 - 2 * (q % 2)
    qy = q + 2 - 4 * (q // 2)
    qd = 3 - q

    def dev(si, zi, ci):
        return {"sp": si, "tp": zi * CORES + ci}

    here = dev(s, z, 1 - c)

    def remote(src, dst, ss, rs, where):
        return pltpu.make_async_remote_copy(
            src_ref=src, dst_ref=dst, send_sem=ss, recv_sem=rs,
            device_id=where, device_id_type=pl.DeviceIdType.MESH)

    def own_tok(u):
        cols = pl.ds(pl.multiple_of((u * CORES + c) * rows, 128), rows)
        return pltpu.make_async_copy(tok.at[0, :, cols], tokens.at[0, u], own_s.at[u])

    def part_tok(u):
        cols = pl.ds(pl.multiple_of((u * CORES + 1 - c) * rows, 128), rows)
        return remote(tok.at[0, :, cols], tokens.at[1, u], tok_s.at[u], tok_r.at[u], here)

    own_wl = pltpu.make_async_copy(wl, wlat.at[z], own_s.at[planes])
    own_wr = pltpu.make_async_copy(wr, wrope.at[z], own_s.at[planes + 1])
    place = pl.ds(pl.multiple_of(s * span, 128), span)
    get_k = pltpu.make_async_copy(kup, kbuf, up_s.at[0])
    get_v = pltpu.make_async_copy(vup, vbuf, up_s.at[1])
    get_c = pltpu.make_async_copy(cos_hbm.at[:, place], cos_ref, up_s.at[2])
    get_n = pltpu.make_async_copy(sin_hbm.at[:, place], sin_ref, up_s.at[3])
    own_wl.start()
    own_wr.start()

    barrier = pltpu.get_barrier_semaphore()

    def greet(where):
        pl.semaphore_signal(barrier, inc=1, device_id=where, device_id_type=pl.DeviceIdType.MESH)

    for i in range(1, planes):
        greet(dev(s, lax.rem(z + i, planes), c))
    for i in range(1, spots):
        greet(dev(lax.rem(s + i, spots), z, c))
    greet(here)
    for u in range(planes):
        own_tok(u).start()
    own_wl.wait()
    own_wr.wait()
    pl.semaphore_wait(barrier, planes - 1 + spots - 1 + 1)

    def piece(u, part, k, ss, rs, where):
        rng = pl.ds(pl.multiple_of(part * quarter + k * eighth, 16), eighth)
        out = [remote(wlat.at[u, rng], wlat.at[u, rng], ss.at[k, u], rs.at[k, u], where)]
        if k == 0:
            rng = pl.ds(pl.multiple_of(part * rpart, 16), rpart)
            out.append(remote(wrope.at[u, rng], wrope.at[u, rng], ss.at[2, u], rs.at[2, u], where))
        return out

    def each(copies, what):
        for p in copies:
            getattr(p, what)()

    def z_rows(k):
        start = q * quarter + k * eighth if k < 2 else qd * quarter + eighth
        return pl.ds(pl.multiple_of(start, 16), eighth)

    def z_piece(u, k, sems, where):
        rng = z_rows(k)
        i = k if k < 2 else 3
        out = [remote(wlat.at[u, rng], wlat.at[u, rng], sems(i), z_r.at[i, u], where)]
        if k == 0:
            rng = pl.ds(pl.multiple_of(q * rpart, 16), rpart)
            out.append(remote(wrope.at[u, rng], wrope.at[u, rng], sems(2), z_r.at[2, u], where))
        return out

    def z_own(k):
        return z_piece(z, k, lambda i: zo_s.at[i], dev(s, z + 1, c))

    def z_up(u, k):
        return z_piece(u, k, lambda i: z_s.at[i, u], dev(s, z + 1, c))

    def z_down(u, k):
        return z_piece(u, k, lambda i: z_s.at[i, u], dev(s, z - 1, c))

    def z_in(u, k):
        return z_piece(u, k, lambda i: z_s.at[i, u], here)

    def by_y(u):
        return (u + c) % 2 == 0

    def x_copy(u, k):
        return piece(u, q, k, x_s, x_r, dev(sx, z, c))

    def y_copy(u, k):
        return piece(u, q, k, y_s, y_r, dev(sy, z, c))

    def x_in(u, k):
        return piece(u, qx, k, x_s, x_r, here)

    def y_in(u, k):
        return piece(u, qy, k, y_s, y_r, here)

    def dy_copy(u):
        return piece(u, qx, 0, dy_s, dy_r, dev(sy, z, c))

    def dx_copy(u):
        return piece(u, qy, 0, dx_s, dx_r, dev(sx, z, c))

    def dy_in(u):
        return piece(u, qd, 0, dy_s, dy_r, here)

    def dx_in(u):
        return piece(u, qd, 0, dx_s, dx_r, here)

    has_up = z + 1 < planes
    has_down = z > 0
    for k in range(2):
        @pl.when(has_up)
        def _():
            each(z_own(k), "start")

        @pl.when(has_down)
        def _():
            each(z_down(z, k), "start")

    for u in range(planes):
        part_tok(u).start()
    get_k.start()
    get_v.start()
    get_c.start()
    get_n.start()
    contract = (((1,), (1,)), ((), ()))

    def block_dot(u):
        x = tokens[:, u].reshape(CORES * span, rows)
        return (jnp.dot(x, wlat[u], preferred_element_type=F32),
                lax.dot_general(wrope[u], x, contract, preferred_element_type=F32))

    def own_block():
        for u in range(planes):
            own_tok(u).wait()
            part_tok(u).wait()
        a, b = block_dot(z)
        acc[...] = a
        acct[...] = b

    put_up = pltpu.make_async_copy(upbuf, up_out, up_s.at[4])

    def reshape_up():
        get_k.wait()
        get_v.wait()
        get_c.wait()
        get_n.wait()
        heads, kw = kbuf.shape[1:]
        vw = vbuf.shape[2]
        k = kbuf[...].astype(F32)
        v = vbuf[...].astype(F32)
        for h in range(heads):
            upbuf[:, h * kw:(h + 1) * kw] = k[:, h, :].astype(BF16)
            upbuf[:, heads * kw + h * vw:heads * kw + (h + 1) * vw] = v[:, h, :].astype(BF16)
        put_up.start()

    def relay(u, k, sign):
        each(z_in(u, k), "wait_recv")
        if sign < 0:
            @pl.when(has_up)
            def _():
                each(z_up(u, k), "start")
        else:
            @pl.when(has_down)
            def _():
                each(z_down(u, k), "start")

    def send_own(k):
        @pl.when(has_up)
        def _():
            each(z_own(k), "start")

        @pl.when(has_down)
        def _():
            each(z_down(z, k), "start")

    def valid(u):
        return (u >= 0) & (u < planes)

    def step(d, carry):
        for k in range(2):
            for sign in (-1, 1):
                u = z + sign * d

                @pl.when(valid(u))
                def _():
                    relay(u, k, sign)
                    each(x_copy(u, k), "start")
                    each(y_copy(u, k), "start")

        @pl.when(d == 1)
        def _():
            own_block()

        @pl.when(d == 2)
        def _():
            reshape_up()

        @pl.when(d == planes - 1)
        def _():
            send_own(2)

        for sign in (-1, 1):
            u = z + sign * (d - 1)

            @pl.when(valid(u) & (d > 1))
            def _():
                @pl.when(by_y(u))
                def _():
                    each(x_in(u, 0), "wait_recv")
                    each(dy_copy(u), "start")

                @pl.when(~by_y(u))
                def _():
                    each(y_in(u, 0), "wait_recv")
                    each(dx_copy(u), "start")
        return carry

    lax.fori_loop(1, planes + 1, step, 0)

    def finish(d, carry):
        for sign in (-1, 1):
            u = z + sign * d

            @pl.when(valid(u))
            def _():
                relay(u, 2, sign)
        for sign in (-1, 1):
            u = z + sign * d

            @pl.when(valid(u))
            def _():
                each(x_in(u, 1), "wait_recv")
                each(y_in(u, 1), "wait_recv")

                @pl.when(by_y(u))
                def _():
                    each(y_in(u, 0), "wait_recv")
                    each(dy_in(u), "wait_recv")

                @pl.when(~by_y(u))
                def _():
                    each(x_in(u, 0), "wait_recv")
                    each(dx_in(u), "wait_recv")
                a, b = block_dot(u)
                acc[...] += a
                acct[...] += b
        return carry

    lax.fori_loop(1, planes, finish, 0)

    swaps = [remote(acc.at[pl.ds(span, span)], other, acc_s.at[0], acc_r.at[0], here),
             remote(acct.at[:, pl.ds(span, span)], othert, acc_s.at[1], acc_r.at[1], here)]
    each(swaps, "start")
    each(swaps, "wait")
    latent = acc[:span] + other[...]
    ropes = acct[:, :span] + othert[...]
    scaled = latent * lax.rsqrt(jnp.mean(latent * latent, axis=-1, keepdims=True) + 1e-06)
    spread[z] = (scaled * scale[...]).astype(BF16)
    swapped = jnp.concatenate([ropes[rope // 2:], ropes[:rope // 2]], axis=0)
    spreadt[z] = (ropes * cos_ref[...] + swapped * sin_ref[...]).astype(BF16)

    def g_copy(u, k, zi, slot):
        rng = pl.ds(k * half, half)
        out = [remote(spread.at[u, rng], spread.at[u, rng], g_s.at[slot, k, u], g_r.at[k, u], dev(s, zi, c))]
        if k == 0:
            out.append(remote(spreadt.at[u], spreadt.at[u], g_s.at[slot, PARTS, u], g_r.at[PARTS, u], dev(s, zi, c)))
        return out

    def lanes(si):
        return pl.ds(pl.multiple_of(si * span, 128), span)

    def f_copy(u, k, where, si):
        rng = pl.ds(k * half, half)
        out = [remote(spread.at[u, rng], x_out.at[c, si, rng], f_s.at[k, u], f_r.at[k, si], where)]
        if k == 0:
            out.append(remote(spreadt.at[u], rot_out.at[c, :, lanes(si)], f_s.at[PARTS, u], f_r.at[PARTS, si], where))
        return out

    def p_copy(ci, si, k):
        rng = pl.ds(k * half, half)
        out = [remote(x_out.at[ci, si, rng], x_out.at[ci, si, rng], p_s.at[k, si], p_r.at[k, si], here)]
        if k == 0:
            part = rot_out.at[ci, :, lanes(si)]
            out.append(remote(part, part, p_s.at[PARTS, si], p_r.at[PARTS, si], here))
        return out

    own_copies = [pltpu.make_async_copy(spread.at[s], x_out.at[c, s], own_s.at[0]),
                  pltpu.make_async_copy(spreadt.at[s], rot_out.at[c, :, lanes(s)], own_s.at[1])]

    def deliver(u, k):
        @pl.when(u != s)
        def _():
            each(f_copy(u, k, dev(u, z, c), s), "start")

        if k == PARTS - 1:
            @pl.when(u == s)
            def _():
                each(own_copies, "start")

    for k in range(PARTS):
        @pl.when(has_up)
        def _():
            each(g_copy(z, k, z + 1, 0), "start")

        @pl.when(has_down)
        def _():
            each(g_copy(z, k, z - 1, 1), "start")

        deliver(z, k)

    def g_step(d, carry):
        for k in range(PARTS):
            for sign in (-1, 1):
                u = z + sign * d

                @pl.when((u >= 0) & (u < planes))
                def _():
                    each(g_copy(u, k, z, 0), "wait_recv")
                    if sign < 0:
                        @pl.when(has_up)
                        def _():
                            each(g_copy(u, k, z + 1, 0), "start")
                    else:
                        @pl.when(has_down)
                        def _():
                            each(g_copy(u, k, z - 1, 1), "start")
                    deliver(u, k)
        return carry

    lax.fori_loop(1, planes, g_step, 0)
    each(own_copies, "wait")
    for k in range(PARTS):
        each(p_copy(c, s, k), "start")

    for k in range(PARTS):
        def p_step(i, carry):
            si = lax.rem(s + i, spots)
            each(f_copy(0, k, here, si), "wait_recv")
            each(p_copy(c, si, k), "start")
            return carry

        lax.fori_loop(1, spots, p_step, 0)

    def p_drain(si, carry):
        for k in range(PARTS):
            each(p_copy(1 - c, si, k), "wait_recv")
            each(p_copy(c, si, k), "wait_send")
        return carry

    lax.fori_loop(0, spots, p_drain, 0)

    def drain(u, carry):
        for k in range(PARTS):
            @pl.when(u != s)
            def _():
                each(f_copy(u, k, here, s), "wait_send")

            @pl.when((u <= z) & has_up)
            def _():
                each(g_copy(u, k, z, 0), "wait_send")

            @pl.when((u >= z) & has_down)
            def _():
                each(g_copy(u, k, z, 1), "wait_send")

        for k in range(3):
            @pl.when((u >= z) & has_down)
            def _():
                each(z_down(u, k), "wait_send")

            @pl.when((u < z) & has_up)
            def _():
                each(z_up(u, k), "wait_send")

        for k in range(2):
            @pl.when(u != z)
            def _():
                each(x_copy(u, k), "wait_send")
                each(y_copy(u, k), "wait_send")

        @pl.when((u != z) & by_y(u))
        def _():
            each(dy_copy(u), "wait_send")

        @pl.when((u != z) & ~by_y(u))
        def _():
            each(dx_copy(u), "wait_send")
        return carry

    lax.fori_loop(0, planes, drain, 0)
    put_up.wait()

    @pl.when(has_up)
    def _():
        for k in range(3):
            each(z_own(k), "wait_send")


def read_kernel(x_ref, r_ref, up_ref, q_ref, cos_ref, sin_ref, plain_ref, value_ref, rot_ref, read_ref, wide):
    length = x_ref.shape[1]
    heads = q_ref.shape[1]
    lat = up_ref.shape[0]
    rope = r_ref.shape[1]
    kw = q_ref.shape[2] - rope
    vw = up_ref.shape[1] // heads - kw
    rotated = r_ref[0]
    rot_ref[0] = rotated
    normed = x_ref[0]
    keys = jnp.dot(normed, up_ref[:, :heads * kw], preferred_element_type=F32)
    values = jnp.dot(normed, up_ref[:, heads * kw:], preferred_element_type=F32)
    for h in range(heads):
        wide[pl.ds(h, length, stride=heads), :] = keys[:, h * kw:(h + 1) * kw]
    plain_ref[0] = wide[...].astype(BF16)
    for h in range(heads):
        wide[pl.ds(h, length, stride=heads), :] = values[:, h * vw:(h + 1) * vw]
    value_ref[0] = wide[...].astype(BF16)
    keys = keys.astype(BF16)
    values = values.astype(BF16)
    query = q_ref[0].astype(F32)
    turned = turn(query[:, kw:], cos_ref[...], sin_ref[...]).astype(BF16)
    tiled = jnp.concatenate([query[:, :kw]] * heads, axis=1)
    row = lax.broadcasted_iota(jnp.int32, tiled.shape, 0)
    col = lax.broadcasted_iota(jnp.int32, tiled.shape, 1)
    blocked = jnp.where(col // kw == row, tiled, 0.0).astype(BF16)
    contract = (((1,), (1,)), ((), ()))
    scores = lax.dot_general(blocked, keys, contract, preferred_element_type=F32)
    scores = scores + jnp.dot(turned, rotated, preferred_element_type=F32)
    scores = scores * (1.0 / (kw + rope) ** 0.5)
    weights = jnp.exp(scores - jnp.max(scores, axis=-1, keepdims=True))
    total = jnp.sum(weights, axis=-1, keepdims=True)
    mixed = jnp.dot(weights.astype(BF16), values, preferred_element_type=F32) / total
    for h in range(heads):
        read_ref[0, h:h + 1, :] = mixed[h:h + 1, h * vw:(h + 1) * vw].astype(BF16)


def body(planes, spots, tokens, latent_down, rope_weight, norm_scale, key_up, value_up, query):
    span = tokens.shape[1]
    rows, lat = latent_down.shape
    rope = rope_weight.shape[1]
    heads, kw = key_up.shape[1:]
    vw = value_up.shape[2]
    length = spots * span
    cosine, sine = turn_tables(np.arange(length + 1), rope)
    vmem = pl.BlockSpec(memory_space=pltpu.VMEM)
    hbm = pl.BlockSpec(memory_space=pl.ANY)
    dma = pltpu.SemaphoreType.DMA
    x_all, rot_all, up = pl.pallas_call(
        functools.partial(move_kernel, planes, spots),
        out_shape=(jax.ShapeDtypeStruct((CORES, spots, span, lat), BF16),
                   jax.ShapeDtypeStruct((CORES, rope, length), BF16),
                   jax.ShapeDtypeStruct((lat, heads * (kw + vw)), BF16)),
        in_specs=[hbm, hbm, hbm, vmem, hbm, hbm, hbm, hbm],
        out_specs=(vmem, vmem, hbm),
        scratch_shapes=[
            pltpu.VMEM((CORES, planes, span, rows), BF16),
            pltpu.VMEM((planes, rows, lat), BF16),
            pltpu.VMEM((planes, rope, rows), BF16),
            pltpu.VMEM((CORES * span, lat), F32),
            pltpu.VMEM((rope, CORES * span), F32),
            pltpu.VMEM((span, lat), F32),
            pltpu.VMEM((rope, span), F32),
            pltpu.VMEM((planes, span, lat), BF16),
            pltpu.VMEM((planes, rope, span), BF16),
            pltpu.VMEM(key_up.shape, BF16),
            pltpu.VMEM(value_up.shape, BF16),
            pltpu.VMEM((lat, heads * (kw + vw)), BF16),
            pltpu.VMEM((rope, span), F32),
            pltpu.VMEM((rope, span), F32),
            dma((planes,)), dma((planes,)), dma((planes + 2,)),
            dma((4, planes)), dma((4, planes)), dma((4,)),
            dma((3, planes)), dma((3, planes)), dma((3, planes)), dma((3, planes)),
            dma((3, planes)), dma((3, planes)), dma((3, planes)), dma((3, planes)),
            dma((2,)), dma((2,)),
            dma((2, PARTS + 1, planes)), dma((PARTS + 1, planes)),
            dma((PARTS + 1, planes)), dma((PARTS + 1, spots)),
            dma((PARTS + 1, spots)), dma((PARTS + 1, spots)),
            dma((5,)),
        ],
        compiler_params=pltpu.CompilerParams(collective_id=0, has_side_effects=True),
    )(tokens, latent_down, rope_weight.T, norm_scale.reshape(1, lat),
      jnp.asarray(np.ascontiguousarray(cosine[:length].T)), jnp.asarray(np.ascontiguousarray(sine[:length].T)),
      key_up, value_up)
    x_all = x_all.reshape(CORES, length, lat)

    def whole(shape):
        return pl.BlockSpec(shape, lambda i: (0,) * len(shape))

    def per(shape):
        return pl.BlockSpec((1,) + shape, lambda i: (i,) + (0,) * len(shape))

    plain, value, rot, read = pl.pallas_call(
        read_kernel,
        grid=(CORES,),
        out_shape=(jax.ShapeDtypeStruct((CORES, length * heads, kw), BF16),
                   jax.ShapeDtypeStruct((CORES, length * heads, vw), BF16),
                   jax.ShapeDtypeStruct((CORES, rope, length), BF16),
                   jax.ShapeDtypeStruct((CORES, heads, vw), BF16)),
        in_specs=[per((length, lat)), per((rope, length)), whole(up.shape), per(query.shape[1:]), whole((1, rope)), whole((1, rope))],
        out_specs=(per((length * heads, kw)), per((length * heads, vw)), per((rope, length)), per((heads, vw))),
        scratch_shapes=[pltpu.VMEM((length * heads, kw), F32)],
    )(x_all, rot_all, up, query, jnp.asarray(cosine[length:]), jnp.asarray(sine[length:]))
    return (plain.reshape(CORES, length, heads, kw), value.reshape(CORES, length, heads, vw), jnp.swapaxes(rot, 1, 2), read)


def solution(mesh):
    planes = mesh.shape["tp"] // CORES
    spots = mesh.shape["sp"]
    assert planes == spots and spots % 4 == 0
    in_specs = (
        P("tp", "sp", None),
        P("tp", None),
        P("tp", None),
        P(),
        P(None, "tp", None),
        P(None, "tp", None),
        P("sp", "tp", None),
    )
    out_specs = (
        P("sp", None, "tp", None),
        P("sp", None, "tp", None),
        P("sp", None, None),
        P("sp", "tp", None),
    )
    return jax.shard_map(functools.partial(body, planes, spots), mesh=mesh, in_specs=in_specs,
                         out_specs=out_specs, check_vma=False)
```

profile of v0, /device:TPU:31, one launch (start us, length us, event | category | flops | bytes accessed | tf_op | source)
XLA Modules:
  0.0 205.6 jit_solution(6158500421623980965)
XLA Ops:
  0.6 1.3 copy.17.q_ref
  1.9 1.8 copy.15.kup
  3.7 1.8 copy.16.vup
  5.5 192.7 %shard_map.138 = (bf16[2,16,128,512]{3,2,1,0:T(8,128)(2,1)}, bf16[2,64,2048]{2,1,0:T(8,128)(2,1)}, bf16[512,256]{1,0:T(8,128)(2,1)}) custom-call(bf16[1,128,4096]{2,1,0:T(8,128)(2,1)} %tok.1, bf16[128,512]{1,0:T(8,128)(2,1)} %wl.1, bf16[64,128]{1,0:T(8,128)(2,1)} %bitcast.11, f32[1,512]{1,0:T(1,128)} %bitcast.12, f32[64,2048]{1,0:T(8,128)} %constant.8.clone.cos_hbm, ...), custom_call_target="tpu_custom_call" | custom-call | tf_op jit(solution)/shard_map/pallas_call | solution.py:501
  198.2 6.2 %shard_map.139 = (bf16[2,2048,128]{2,1,0:T(8,128)(2,1)}, bf16[2,2048,128]{2,1,0:T(8,128)(2,1)}, bf16[2,64,2048]{2,1,0:T(8,128)(2,1)}, bf16[2,1,128]{2,1,0:T(2,128)(2,1)}) custom-call(bf16[2,2048,512]{2,1,0:T(8,128)(2,1)} %bitcast.10, bf16[2,64,2048]{2,1,0:T(8,128)(2,1)} %get-tuple-element.12.r_ref, bf16[512,256]{1,0:T(8,128)(2,1)} %get-tuple-element.13.up_ref, ...), custom_call_target="tpu_custom_call" | custom-call | tf_op jit(solution)/shard_map/pallas_call | solution.py:545
  204.4 1.2 copy.20
where the time goes:
time: 206 us
  Pallas kernels  199 us (97%)
  local copies, waits for them, and re-layouts  6.08 us (3%)
    pallas_call x1, Pallas kernels, body(): pl.pallas_call(functools.partial(move_kernel, planes, spots), out_shape=(...  193 us
    pallas_call x1, Pallas kernels, body(): pl.pallas_call(read_kernel, grid=(CORES,), out_shape=(jax.ShapeDtypeStruc...  6.19 us
    unnamed x4, local copies, waits for them, and re-layouts  6.08 us

commit v1 on v0

v1 whole, which is shorter than its diff:
```python
import functools

import numpy as np
import jax
import jax.numpy as jnp
from jax import lax
from jax.sharding import PartitionSpec as P
from jax.experimental import pallas as pl
from jax.experimental.pallas import tpu as pltpu

CORES = 2
SIDE = 4
PARTS = 4
BF16 = jnp.bfloat16
F32 = jnp.float32


def turn_tables(positions, width):
    half = width // 2
    freqs = (1.0 / np.float32(10000.0) ** (np.arange(half, dtype=np.float32) * np.float32(2.0) / np.float32(width))).astype(np.float32)
    angles = positions.astype(np.float32)[:, None] * freqs
    cosine = np.cos(angles).astype(np.float32)
    sine = np.sin(angles).astype(np.float32)
    return np.concatenate([cosine, cosine], -1), np.concatenate([-sine, sine], -1)


def turn(part, cosine, sine):
    half = part.shape[-1] // 2
    swapped = jnp.concatenate([part[:, half:], part[:, :half]], axis=-1)
    return part * cosine + swapped * sine


def move_kernel(planes, spots, tok, wl, wr, scale, cos_hbm, sin_hbm, fin, fint,
                tokens, wlat, wrope, acc, acct, other, othert, own, ownt, trans, transt, cos_ref, sin_ref,
                tok_s, tok_r, own_s, z_s, z_r, a_s, a_r, b_s, b_r, t_s, t_r,
                acc_s, acc_r, x_s, x_r, up_s, down_s, in_r, y_s, y_r, p_s, p_r):
    s = lax.axis_index("sp")
    t = lax.axis_index("tp")
    z = t // CORES
    c = t % CORES
    x = s % SIDE
    y = s // SIDE
    rows, lat = wl.shape
    rope = wr.shape[0]
    span = tok.shape[1]
    rcut = rows // SIDE
    lcut = lat // SIDE
    pcut = rope // SIDE
    cut = span // PARTS
    far = planes // 2

    def dev(yi, xi, zi, ci):
        return {"sp": yi * SIDE + xi, "tp": zi * CORES + ci}

    here = dev(y, x, z, 1 - c)

    def around(v, n):
        return lax.rem(v + n, n)

    def remote(src, dst, ss, rs, where):
        return pltpu.make_async_remote_copy(
            src_ref=src, dst_ref=dst, send_sem=ss, recv_sem=rs,
            device_id=where, device_id_type=pl.DeviceIdType.MESH)

    def each(copies, what):
        for p in copies:
            getattr(p, what)()

    def own_tok(u):
        cols = pl.ds(pl.multiple_of((u * CORES + c) * rows, 128), rows)
        return pltpu.make_async_copy(tok.at[0, :, cols], tokens.at[0, u], own_s.at[u])

    def part_tok(u):
        cols = pl.ds(pl.multiple_of((u * CORES + 1 - c) * rows, 128), rows)
        return remote(tok.at[0, :, cols], tokens.at[1, u], tok_s.at[u], tok_r.at[u], here)

    own_wl = pltpu.make_async_copy(wl, wlat.at[z], own_s.at[planes])
    own_wr = pltpu.make_async_copy(wr, wrope.at[z], own_s.at[planes + 1])
    place = pl.ds(pl.multiple_of(s * span, 128), span)
    get_c = pltpu.make_async_copy(cos_hbm.at[:, place], cos_ref, own_s.at[planes + 2])
    get_n = pltpu.make_async_copy(sin_hbm.at[:, place], sin_ref, own_s.at[planes + 3])
    own_wl.start()
    own_wr.start()

    barrier = pltpu.get_barrier_semaphore()

    def greet(where):
        pl.semaphore_signal(barrier, inc=1, device_id=where, device_id_type=pl.DeviceIdType.MESH)

    for i in range(1, planes):
        greet(dev(y, x, around(z + i, planes), c))
    for i in range(1, SIDE):
        greet(dev(y, around(x + i, SIDE), z, c))
        greet(dev(around(y + i, SIDE), x, z, c))
    greet(here)
    for u in range(planes):
        own_tok(u).start()
    get_c.start()
    get_n.start()
    own_wl.wait()
    own_wr.wait()
    pl.semaphore_wait(barrier, planes - 1 + 2 * (SIDE - 1) + 1)

    def w_piece(u):
        return wlat.at[u, pl.ds(pl.multiple_of(y * rcut, 16), rcut), pl.ds(pl.multiple_of(x * lcut, 128), lcut)]

    def w_row(u):
        return wlat.at[u, pl.ds(pl.multiple_of(y * rcut, 16), rcut)]

    def w_col(u):
        return wlat.at[u, :, pl.ds(pl.multiple_of(x * lcut, 128), lcut)]

    def r_piece(u, i):
        return wrope.at[u, pl.ds(pl.multiple_of(i * pcut, 16), pcut)]

    def z_copy(u, zi, i):
        where = dev(y, x, zi, c)
        return [remote(w_piece(u), w_piece(u), z_s.at[0, zi], z_r.at[0, u], where),
                remote(r_piece(u, i), r_piece(u, i), z_s.at[1, zi], z_r.at[1, u], where)]

    def a_copy(u, o, by_row):
        where = dev(y, around(x + o, SIDE), z, c) if by_row else dev(around(y + o, SIDE), x, z, c)
        return remote(w_piece(u), w_piece(u), a_s.at[o - 1, u], a_r.at[o - 1, u], where)

    def b_copy(u, o, by_row):
        where = dev(around(y + o, SIDE), x, z, c) if by_row else dev(y, around(x + o, SIDE), z, c)
        part = w_row(u) if by_row else w_col(u)
        turned = r_piece(u, y if by_row else x)
        return [remote(part, part, b_s.at[o - 1, u], b_r.at[o - 1, u], where),
                remote(turned, turned, t_s.at[o - 1, u], t_r.at[o - 1, u], where)]

    def below(d):
        return around(z - d, planes)

    def above(d):
        return around(z + d, planes)

    def z_send(d, carry):
        each(z_copy(z, above(d), y), "start")

        @pl.when(d < far)
        def _():
            each(z_copy(z, below(d), x), "start")
        return carry

    lax.fori_loop(1, far + 1, z_send, 0)
    for u in range(planes):
        part_tok(u).start()

    contract = (((1,), (1,)), ((), ()))

    def block_dot(u):
        v = tokens[:, u].reshape(CORES * span, rows)
        return (jnp.dot(v, wlat[u], preferred_element_type=F32),
                lax.dot_general(wrope[u], v, contract, preferred_element_type=F32))

    def own_block():
        for u in range(planes):
            own_tok(u).wait()
            part_tok(u).wait()
        a, b = block_dot(z)
        acc[...] = a
        acct[...] = b

    def first(u, by_row):
        z_copy(u, z, y)[0].wait_recv()
        for o in range(1, SIDE):
            a_copy(u, o, by_row).start()

    def second(u, by_row):
        z_copy(u, z, y)[1].wait_recv()
        for o in range(1, SIDE):
            a_copy(u, o, by_row).wait_recv()
        for o in range(1, SIDE):
            each(b_copy(u, o, by_row), "start")

    def third(u, by_row):
        for o in range(1, SIDE):
            each(b_copy(u, o, by_row), "wait_recv")
        a, b = block_dot(u)
        acc[...] += a
        acct[...] += b

    def both(d, what):
        @pl.when((d >= 1) & (d <= far))
        def _():
            what(below(d), True)

        @pl.when((d >= 1) & (d < far))
        def _():
            what(above(d), False)

    def step(i, carry):
        both(i, first)
        both(i - 2, second)

        @pl.when(i == 3)
        def _():
            own_block()

        both(i - 4, third)
        return carry

    lax.fori_loop(1, far + 5, step, 0)

    swaps = [remote(acc.at[pl.ds(span, span)], other, acc_s.at[0], acc_r.at[0], here),
             remote(acct.at[:, pl.ds(span, span)], othert, acc_s.at[1], acc_r.at[1], here)]
    each(swaps, "start")
    get_c.wait()
    get_n.wait()
    each(swaps, "wait")
    latent = acc[:span] + other[...]
    ropes = acct[:, :span] + othert[...]
    scaled = latent * lax.rsqrt(jnp.mean(latent * latent, axis=-1, keepdims=True) + 1e-06)
    normed = (scaled * scale[...]).astype(BF16)
    swapped = jnp.concatenate([ropes[rope // 2:], ropes[:rope // 2]], axis=0)
    rotated = (ropes * cos_ref[...] + swapped * sin_ref[...]).astype(BF16)

    xq = z % SIDE
    kq = z // SIDE
    origin = x == xq

    @pl.when(origin)
    def _():
        trans[kq * SIDE + x] = normed
        transt[kq * SIDE + x] = rotated

    @pl.when(~origin)
    def _():
        own[...] = normed
        ownt[...] = rotated

    def chunk(p):
        return pl.ds(p * cut, cut)

    def x_copy(xs, p):
        slot = kq * SIDE + xs
        where = dev(y, xq, z, c)
        out = [remote(own.at[chunk(p)], trans.at[slot, chunk(p)], x_s.at[p], x_r.at[p, xs], where)]
        if p == 0:
            out.append(remote(ownt, transt.at[slot], x_s.at[PARTS], x_r.at[PARTS, xs], where))
        return out

    def z_move(slot, p, zi, sems):
        where = dev(y, x, zi, c)
        out = [remote(trans.at[slot, chunk(p)], trans.at[slot, chunk(p)], sems.at[p, slot], in_r.at[p, slot], where)]
        if p == 0:
            out.append(remote(transt.at[slot], transt.at[slot], sems.at[PARTS, slot], in_r.at[PARTS, slot], where))
        return out

    def up_move(slot, p):
        return z_move(slot, p, around(z + 1, planes), up_s)

    def down_move(slot, p):
        return z_move(slot, p, around(z - 1, planes), down_s)

    def y_move(k, xs, p, place):
        slot = k * SIDE + xs
        where = dev(k, x, z, c)
        out = [remote(trans.at[slot, chunk(p)], fin.at[c, place, chunk(p)], y_s.at[p, slot], y_r.at[p, place], where)]
        if p == 0:
            out.append(remote(transt.at[slot], fint.at[c, place], y_s.at[PARTS, slot], y_r.at[PARTS, place], where))
        return out

    def p_from(src, srct, place, p):
        out = [remote(src, fin.at[c, place, chunk(p)], p_s.at[p, place], p_r.at[p, place], here)]
        if p == 0:
            out.append(remote(srct, fint.at[c, place], p_s.at[PARTS, place], p_r.at[PARTS, place], here))
        return out

    def p_pass(place, p):
        return p_from(fin.at[c, place, chunk(p)], fint.at[c, place], place, p)

    def p_keep(xs, p):
        slot = y * SIDE + xs
        return p_from(trans.at[slot, chunk(p)], transt.at[slot], slot, p)

    def p_in(place, p):
        mine = [remote(fin.at[1 - c, place, chunk(p)], fin.at[1 - c, place, chunk(p)], p_s.at[p, place], p_r.at[p, place], here)]
        if p == 0:
            mine.append(remote(fint.at[1 - c, place], fint.at[1 - c, place], p_s.at[PARTS, place], p_r.at[PARTS, place], here))
        return mine

    early = PARTS // 2

    def goes_up(f, p):
        return (f < far - 1) | (f == far - 1) if p < early else f < far - 1

    def goes_down(f, p):
        return f < far - 1 if p < early else (f < far - 1) | (f == far - 1)

    def hand_over(k, xs, p):
        @pl.when(k != y)
        def _():
            each(y_move(k, xs, p, y * SIDE + xs), "start")

        @pl.when(k == y)
        def _():
            slot = k * SIDE + xs
            each(p_keep(xs, p), "start")
            fin[c, slot, p * cut:(p + 1) * cut] = trans[slot, p * cut:(p + 1) * cut]
            if p == 0:
                fint[c, slot] = transt[slot]

    @pl.when(~origin)
    def _():
        for p in range(PARTS):
            each(x_copy(x, p), "start")

    e = lax.rem(z - x + planes, SIDE)
    lower = jnp.where(e == 0, SIDE, e)
    upper = SIDE - e

    def ring(i, carry):
        ib = i - lower
        ia = i - upper
        db = lower + SIDE * (ib // SIDE)
        da = upper + SIDE * (ia // SIDE)
        kb = around(z - db, planes) // SIDE
        ka = around(z + da, planes) // SIDE
        xb = lax.rem(ib + SIDE, SIDE)
        xa = lax.rem(ia + SIDE, SIDE)
        for p in range(PARTS):
            @pl.when(origin & (i < SIDE))
            def _():
                xs = lax.rem(x + i, SIDE)
                slot = kq * SIDE + xs

                @pl.when(i > 0)
                def _():
                    each(x_copy(xs, p), "wait_recv")
                each(up_move(slot, p), "start")
                each(down_move(slot, p), "start")
                hand_over(kq, xs, p)

            @pl.when((ib >= 0) & (ib < 2 * SIDE) & ((db < far) | (p < early)))
            def _():
                slot = kb * SIDE + lax.rem(x + xb, SIDE)
                each(up_move(slot, p), "wait_recv")

                @pl.when(goes_up(db, p))
                def _():
                    each(up_move(slot, p), "start")
                hand_over(kb, lax.rem(x + xb, SIDE), p)

            @pl.when((ia >= 0) & (ia < 2 * SIDE) & ((da < far) | (p >= early)))
            def _():
                slot = ka * SIDE + lax.rem(x + xa, SIDE)
                each(down_move(slot, p), "wait_recv")

                @pl.when(goes_down(da, p))
                def _():
                    each(down_move(slot, p), "start")
                hand_over(ka, lax.rem(x + xa, SIDE), p)
        return carry

    lax.fori_loop(0, 3 * SIDE, ring, 0)

    def pass_on(xs, carry):
        for p in range(PARTS):
            for o in range(1, SIDE):
                place = around(y + o, SIDE) * SIDE + xs
                each(y_move(y, xs, p, place), "wait_recv")
                each(p_pass(place, p), "start")
        return carry

    lax.fori_loop(0, SIDE, pass_on, 0)

    def drain(i, carry):
        k = i // SIDE
        xs = lax.rem(i, SIDE)
        u = x + k * SIDE
        f = around(z - u, planes)
        g = around(u - z, planes)
        for p in range(PARTS):
            each(p_in(i, p), "wait_recv")
            each(p_pass(i, p), "wait_send")

            @pl.when(goes_up(f, p))
            def _():
                each(up_move(i, p), "wait_send")

            @pl.when(goes_down(g, p))
            def _():
                each(down_move(i, p), "wait_send")

            @pl.when(k != y)
            def _():
                each(y_move(k, xs, p, y * SIDE + xs), "wait_send")
        return carry

    lax.fori_loop(0, spots, drain, 0)

    @pl.when(~origin)
    def _():
        for p in range(PARTS):
            each(x_copy(x, p), "wait_send")

    def settle(d, carry):
        each(z_copy(z, above(d), y), "wait_send")

        def sent(u, by_row):
            for o in range(1, SIDE):
                a_copy(u, o, by_row).wait_send()
                each(b_copy(u, o, by_row), "wait_send")

        sent(below(d), True)

        @pl.when(d < far)
        def _():
            each(z_copy(z, below(d), x), "wait_send")
            sent(above(d), False)
        return carry

    lax.fori_loop(1, far + 1, settle, 0)


def read_kernel(x_ref, r_ref, k_ref, v_ref, q_ref, cos_ref, sin_ref, plain_ref, value_ref, rot_ref, read_ref):
    spots, rope, span = r_ref.shape[1:]
    kw = k_ref.shape[1]
    for i in range(spots):
        rot_ref[0, :, i * span:(i + 1) * span] = r_ref[0, i]
    normed = x_ref[0]
    keys = jnp.dot(normed, k_ref[...], preferred_element_type=F32).astype(BF16)
    values = jnp.dot(normed, v_ref[...], preferred_element_type=F32).astype(BF16)
    plain_ref[0] = keys
    value_ref[0] = values
    part = pl.program_id(0)
    both = q_ref[...].astype(F32)
    query = jnp.where(part == 0, both[:1], both[1:])
    turned = turn(query[:, kw:], cos_ref[...], sin_ref[...]).astype(BF16)
    contract = (((1,), (1,)), ((), ()))
    scores = lax.dot_general(query[:, :kw].astype(BF16), keys, contract, preferred_element_type=F32)
    scores = scores + jnp.dot(turned, rot_ref[0], preferred_element_type=F32)
    scores = scores * (1.0 / (kw + rope) ** 0.5)
    weights = jnp.exp(scores - jnp.max(scores, axis=-1, keepdims=True))
    total = jnp.sum(weights, axis=-1, keepdims=True)
    mixed = jnp.dot(weights.astype(BF16), values, preferred_element_type=F32) / total
    spot = lax.broadcasted_iota(jnp.int32, read_ref.shape, 0)
    kept = jnp.where(spot == part, mixed, read_ref[...].astype(F32))
    read_ref[...] = jnp.where((part > 0) | (spot == 0), kept, 0.0).astype(BF16)


def body(planes, spots, tokens, latent_down, rope_weight, norm_scale, key_up, value_up, query):
    span = tokens.shape[1]
    rows, lat = latent_down.shape
    rope = rope_weight.shape[1]
    heads, kw = key_up.shape[1:]
    vw = value_up.shape[2]
    assert heads == 1
    length = spots * span
    cosine, sine = turn_tables(np.arange(length + 1), rope)
    vmem = pl.BlockSpec(memory_space=pltpu.VMEM)
    hbm = pl.BlockSpec(memory_space=pl.ANY)
    dma = pltpu.SemaphoreType.DMA
    x_all, rot_all = pl.pallas_call(
        functools.partial(move_kernel, planes, spots),
        out_shape=(jax.ShapeDtypeStruct((CORES, spots, span, lat), BF16),
                   jax.ShapeDtypeStruct((CORES, spots, rope, span), BF16)),
        in_specs=[hbm, hbm, hbm, vmem, hbm, hbm],
        out_specs=(vmem, vmem),
        scratch_shapes=[
            pltpu.VMEM((CORES, planes, span, rows), BF16),
            pltpu.VMEM((planes, rows, lat), BF16),
            pltpu.VMEM((planes, rope, rows), BF16),
            pltpu.VMEM((CORES * span, lat), F32),
            pltpu.VMEM((rope, CORES * span), F32),
            pltpu.VMEM((span, lat), F32),
            pltpu.VMEM((rope, span), F32),
            pltpu.VMEM((span, lat), BF16),
            pltpu.VMEM((rope, span), BF16),
            pltpu.VMEM((spots, span, lat), BF16),
            pltpu.VMEM((spots, rope, span), BF16),
            pltpu.VMEM((rope, span), F32),
            pltpu.VMEM((rope, span), F32),
            dma((planes,)), dma((planes,)), dma((planes + 4,)),
            dma((2, planes)), dma((2, planes)),
            dma((SIDE - 1, planes)), dma((SIDE - 1, planes)),
            dma((SIDE - 1, planes)), dma((SIDE - 1, planes)),
            dma((SIDE - 1, planes)), dma((SIDE - 1, planes)),
            dma((2,)), dma((2,)),
            dma((PARTS + 1,)), dma((PARTS + 1, SIDE)),
            dma((PARTS + 1, spots)), dma((PARTS + 1, spots)), dma((PARTS + 1, spots)),
            dma((PARTS + 1, spots)), dma((PARTS + 1, spots)),
            dma((PARTS + 1, spots)), dma((PARTS + 1, spots)),
        ],
        compiler_params=pltpu.CompilerParams(collective_id=0, has_side_effects=True),
    )(tokens, latent_down, rope_weight.T, norm_scale.reshape(1, lat),
      jnp.asarray(np.ascontiguousarray(cosine[:length].T)), jnp.asarray(np.ascontiguousarray(sine[:length].T)))
    x_all = x_all.reshape(CORES, length, lat)

    def whole(shape):
        return pl.BlockSpec(shape, lambda i: (0,) * len(shape))

    def per(shape):
        return pl.BlockSpec((1,) + shape, lambda i: (i,) + (0,) * len(shape))

    plain, value, rot, read = pl.pallas_call(
        read_kernel,
        grid=(CORES,),
        out_shape=(jax.ShapeDtypeStruct((CORES, length, kw), BF16),
                   jax.ShapeDtypeStruct((CORES, length, vw), BF16),
                   jax.ShapeDtypeStruct((CORES, rope, length), BF16),
                   jax.ShapeDtypeStruct((CORES, vw), BF16)),
        in_specs=[per((length, lat)), per((spots, rope, span)), whole((lat, kw)), whole((lat, vw)),
                  whole((CORES, query.shape[2])), whole((1, rope)), whole((1, rope))],
        out_specs=(per((length, kw)), per((length, vw)), per((rope, length)), whole((CORES, vw))),
    )(x_all, rot_all, key_up.reshape(lat, kw), value_up.reshape(lat, vw), query.reshape(CORES, -1),
      jnp.asarray(cosine[length:]), jnp.asarray(sine[length:]))
    return (plain.reshape(CORES, length, heads, kw), value.reshape(CORES, length, heads, vw), jnp.swapaxes(rot, 1, 2),
            read.reshape(CORES, heads, vw))


def solution(mesh):
    planes = mesh.shape["tp"] // CORES
    spots = mesh.shape["sp"]
    assert planes == spots == SIDE * SIDE
    in_specs = (
        P("tp", "sp", None),
        P("tp", None),
        P("tp", None),
        P(),
        P(None, "tp", None),
        P(None, "tp", None),
        P("sp", "tp", None),
    )
    out_specs = (
        P("sp", None, "tp", None),
        P("sp", None, "tp", None),
        P("sp", None, None),
        P("sp", "tp", None),
    )
    return jax.shard_map(functools.partial(body, planes, spots), mesh=mesh, in_specs=in_specs,
                         out_specs=out_specs, check_vma=False)
```

time: 206 us -> 116 us (0.56)
  the two profiles are of different devices: /device:TPU:31 before, /device:TPU:51 now
where the time goes in v1:
time: 116 us
  Pallas kernels  115 us (99%)
    pallas_call x1, Pallas kernels, body(): pl.pallas_call(functools.partial(move_kernel, planes, spots), out_shape=(...  109 us
    pallas_call x1, Pallas kernels, body(): pl.pallas_call(read_kernel, grid=(CORES,), out_shape=(jax.ShapeDtypeStruc...  5.73 us

profile of v1, /device:TPU:51, one launch (start us, length us, event | category | flops | bytes accessed | tf_op | source)
XLA Modules:
  0.0 115.6 jit_solution(11744350224035828307)
XLA Ops:
  0.6 109.2 %shard_map.138 = (bf16[2,16,128,512]{3,2,1,0:T(8,128)(2,1)}, bf16[2,16,64,128]{3,2,1,0:T(8,128)(2,1)}) custom-call(bf16[1,128,4096]{2,1,0:T(8,128)(2,1)} %tok.1, bf16[128,512]{1,0:T(8,128)(2,1)} %wl.1, bf16[64,128]{1,0:T(8,128)(2,1)} %bitcast.17, f32[1,512]{1,0:T(1,128)} %bitcast.18, f32[64,2048]{1,0:T(8,128)} %constant.8.clone.cos_hbm, ...), custom_call_target="tpu_custom_call" | custom-call | tf_op jit(solution)/shard_map/pallas_call | solution.py:456
  109.9 5.7 %shard_map.139 = (bf16[2,2048,128]{2,1,0:T(8,128)(2,1)}, bf16[2,2048,128]{2,1,0:T(8,128)(2,1)}, bf16[2,64,2048]{2,1,0:T(8,128)(2,1)}, bf16[2,128]{1,0:T(2,128)(2,1)}) custom-call(bf16[2,2048,512]{2,1,0:T(8,128)(2,1)} %bitcast.14, bf16[2,16,64,128]{3,2,1,0:T(8,128)(2,1)} %get-tuple-element.11.r_ref, bf16[512,128]{1,0:T(8,128)(2,1)} %bitcast.15, ...), custom_call_target="tpu_custom_call" | custom-call | tf_op jit(solution)/shard_map/pallas_call | solution.py:498

commit v2 on v1

v2 whole, which is shorter than its diff:
```python
import functools

import numpy as np
import jax
import jax.numpy as jnp
from jax import lax
from jax.sharding import PartitionSpec as P
from jax.experimental import pallas as pl
from jax.experimental.pallas import tpu as pltpu

CORES = 2
SIDE = 4
PARTS = 3
EARLY = 2
STEPS = 4
GRANT = 61_900_000
READ_GRANT = 40_000_000
BF16 = jnp.bfloat16
F32 = jnp.float32


def turn_tables(positions, width):
    half = width // 2
    freqs = (1.0 / np.float32(10000.0) ** (np.arange(half, dtype=np.float32) * np.float32(2.0) / np.float32(width))).astype(np.float32)
    angles = positions.astype(np.float32)[:, None] * freqs
    cosine = np.cos(angles).astype(np.float32)
    sine = np.sin(angles).astype(np.float32)
    return np.concatenate([cosine, cosine], -1), np.concatenate([-sine, sine], -1)


def turn(part, cosine, sine):
    half = part.shape[-1] // 2
    swapped = jnp.concatenate([part[:, half:], part[:, :half]], axis=-1)
    return part * cosine + swapped * sine


def move_kernel(planes, spots, tok, wl, wr, scale_hbm, cos_hbm, sin_hbm, kup, vup, q_hbm, qcos_hbm, qsin_hbm, fin, up, ask,
                tokens, wlat, wrope, acc, acct, other, othert, own, trans, cos_ref, sin_ref, scale, query, qcos, qsin,
                tok_s, tok_r, tok_o, own_s, z_s, z_r, a_s, a_r, b_s, b_r, t_s, t_r,
                acc_s, acc_r, x_s, x_r, up_s, down_s, in_r, y_s, y_r, p_s, p_r):
    s = lax.axis_index("sp")
    t = lax.axis_index("tp")
    z = t // CORES
    c = t % CORES
    x = s % SIDE
    y = s // SIDE
    rows, lat = wl.shape
    rope = wr.shape[0]
    span = tok.shape[1]
    rcut = rows // SIDE
    lcut = lat // SIDE
    pcut = rope // SIDE
    block = fin.shape[2]
    cut = block // PARTS
    kw = kup.shape[1]
    far = planes // 2

    def dev(yi, xi, zi, ci):
        return {"sp": yi * SIDE + xi, "tp": zi * CORES + ci}

    here = dev(y, x, z, 1 - c)

    def around(v, n):
        return lax.rem(v + n, n)

    def remote(src, dst, ss, rs, where):
        return pltpu.make_async_remote_copy(
            src_ref=src, dst_ref=dst, send_sem=ss, recv_sem=rs,
            device_id=where, device_id_type=pl.DeviceIdType.MESH)

    def each(copies, what):
        for p in copies:
            getattr(p, what)()

    def own_tok(u):
        cols = pl.ds(pl.multiple_of((u * CORES + c) * rows, 128), rows)
        return pltpu.make_async_copy(tok.at[0, :, cols], tokens.at[0, u], tok_o)

    def part_tok(u):
        cols = pl.ds(pl.multiple_of((u * CORES + 1 - c) * rows, 128), rows)
        return remote(tok.at[0, :, cols], tokens.at[1, u], tok_s, tok_r, here)

    own_wl = pltpu.make_async_copy(wl, wlat.at[z], own_s.at[0])
    own_wr = pltpu.make_async_copy(wr, wrope.at[z], own_s.at[1])
    place = pl.ds(pl.multiple_of(s * span, 128), span)
    tables = [pltpu.make_async_copy(cos_hbm.at[:, place], cos_ref, own_s.at[2]),
              pltpu.make_async_copy(sin_hbm.at[:, place], sin_ref, own_s.at[3]),
              pltpu.make_async_copy(scale_hbm, scale, own_s.at[4]),
              pltpu.make_async_copy(q_hbm, query, own_s.at[5]),
              pltpu.make_async_copy(qcos_hbm, qcos, own_s.at[6]),
              pltpu.make_async_copy(qsin_hbm, qsin, own_s.at[7]),
              pltpu.make_async_copy(kup, up.at[:, pl.ds(0, kw)], own_s.at[8]),
              pltpu.make_async_copy(vup, up.at[:, pl.ds(kw, up.shape[1] - kw)], own_s.at[9])]
    own_wl.start()
    own_wr.start()

    barrier = pltpu.get_barrier_semaphore()

    def greet(where):
        pl.semaphore_signal(barrier, inc=1, device_id=where, device_id_type=pl.DeviceIdType.MESH)

    for i in range(1, planes):
        greet(dev(y, x, around(z + i, planes), c))
    for i in range(1, SIDE):
        greet(dev(y, around(x + i, SIDE), z, c))
        greet(dev(around(y + i, SIDE), x, z, c))
    greet(here)
    for u in range(planes):
        own_tok(u).start()
    own_wl.wait()
    own_wr.wait()
    pl.semaphore_wait(barrier, planes - 1 + 2 * (SIDE - 1) + 1)

    def w_piece(u):
        return wlat.at[u, pl.ds(pl.multiple_of(y * rcut, 16), rcut), pl.ds(pl.multiple_of(x * lcut, 128), lcut)]

    def w_row(u):
        return wlat.at[u, pl.ds(pl.multiple_of(y * rcut, 16), rcut)]

    def w_col(u):
        return wlat.at[u, :, pl.ds(pl.multiple_of(x * lcut, 128), lcut)]

    def r_piece(u, i):
        return wrope.at[u, pl.ds(pl.multiple_of(i * pcut, 16), pcut)]

    def z_copy(u, zi, i):
        where = dev(y, x, zi, c)
        return [remote(w_piece(u), w_piece(u), z_s, z_r.at[u], where),
                remote(r_piece(u, i), r_piece(u, i), z_s, z_r.at[u], where)]

    def a_copy(u, o, by_row):
        where = dev(y, around(x + o, SIDE), z, c) if by_row else dev(around(y + o, SIDE), x, z, c)
        return remote(w_piece(u), w_piece(u), a_s, a_r.at[u], where)

    def b_copy(u, o, by_row):
        where = dev(around(y + o, SIDE), x, z, c) if by_row else dev(y, around(x + o, SIDE), z, c)
        part = w_row(u) if by_row else w_col(u)
        turned = r_piece(u, y if by_row else x)
        return [remote(part, part, b_s, b_r.at[u], where),
                remote(turned, turned, t_s, t_r.at[u], where)]

    def arrived(sem, count, deep, wide):
        part = wlat.at[pl.ds(0, count), pl.ds(0, deep), pl.ds(0, wide)]
        pltpu.make_async_copy(part, part, sem).wait()

    def below(d):
        return around(z - d, planes)

    def above(d):
        return around(z + d, planes)

    def z_send(d, carry):
        each(z_copy(z, above(d), y), "start")

        @pl.when(d < far)
        def _():
            each(z_copy(z, below(d), x), "start")
        return carry

    lax.fori_loop(1, far + 1, z_send, 0)
    for u in range(planes):
        part_tok(u).start()
    each(tables, "start")

    contract = (((1,), (1,)), ((), ()))

    def block_dot(u):
        v = tokens[:, u].reshape(CORES * span, rows)
        return (jnp.dot(v, wlat[u], preferred_element_type=F32),
                lax.dot_general(wrope[u], v, contract, preferred_element_type=F32))

    def own_block():
        pltpu.make_async_copy(tokens.at[0], tokens.at[0], tok_o).wait()
        pltpu.make_async_copy(tokens.at[1], tokens.at[1], tok_r).wait()
        a, b = block_dot(z)
        acc[...] = a
        acct[...] = b

    def first(u, by_row):
        arrived(z_r.at[u], 1, rcut + pcut, lcut)
        for o in range(1, SIDE):
            a_copy(u, o, by_row).start()

    def second(u, by_row):
        arrived(a_r.at[u], 1, rcut, lcut * (SIDE - 1))
        for o in range(1, SIDE):
            each(b_copy(u, o, by_row), "start")

    def third(u, by_row):
        arrived(b_r.at[u], 1, rcut * (SIDE - 1), lat)
        arrived(t_r.at[u], 1, pcut, rows * (SIDE - 1))
        a, b = block_dot(u)
        acc[...] += a
        acct[...] += b

    def both(d, what):
        @pl.when((d >= 1) & (d <= far))
        def _():
            what(below(d), True)

        @pl.when((d >= 1) & (d < far))
        def _():
            what(above(d), False)

    def step(i, carry):
        both(i, first)
        both(i - 2, second)

        @pl.when(i == 3)
        def _():
            own_block()

        both(i - 4, third)
        return carry

    lax.fori_loop(1, far + 5, step, 0)

    swaps = [remote(acc.at[pl.ds(span, span)], other, acc_s.at[0], acc_r.at[0], here),
             remote(acct.at[:, pl.ds(span, span)], othert, acc_s.at[1], acc_r.at[1], here)]
    each(swaps, "start")
    each(tables, "wait")
    asked = query[...].astype(F32)
    ask[...] = jnp.concatenate([asked[:, :kw], turn(asked[:, kw:], qcos[...], qsin[...])], axis=1).astype(BF16)
    each(swaps, "wait")
    latent = acc[:span] + other[...]
    ropes = acct[:, :span] + othert[...]
    scaled = latent * lax.rsqrt(jnp.mean(latent * latent, axis=-1, keepdims=True) + 1e-06)
    normed = (scaled * scale[...]).astype(BF16)
    swapped = jnp.concatenate([ropes[rope // 2:], ropes[:rope // 2]], axis=0)
    rotated = (ropes * cos_ref[...] + swapped * sin_ref[...]).astype(BF16)

    xq = z % SIDE
    kq = z // SIDE
    origin = x == xq

    folded = jnp.concatenate([rotated[i * pcut:(i + 1) * pcut] for i in range(SIDE)], axis=1)

    @pl.when(origin)
    def _():
        trans[kq * SIDE + x, :span] = normed
        trans[kq * SIDE + x, span:] = folded

    @pl.when(~origin)
    def _():
        own[:span] = normed
        own[span:] = folded

    def chunk(p):
        return pl.ds(p * cut, cut)

    def x_copy(xs, p):
        slot = kq * SIDE + xs
        return remote(own.at[chunk(p)], trans.at[slot, chunk(p)], x_s, x_r.at[p, xs], dev(y, xq, z, c))

    def z_move(slot, p, zi, sem):
        part = trans.at[slot, chunk(p)]
        return remote(part, part, sem, in_r.at[p, slot], dev(y, x, zi, c))

    def up_move(slot, p):
        return z_move(slot, p, around(z + 1, planes), up_s)

    def down_move(slot, p):
        return z_move(slot, p, around(z - 1, planes), down_s)

    def y_move(k, xs, p, place):
        return remote(trans.at[k * SIDE + xs, chunk(p)], fin.at[c, place, chunk(p)], y_s, y_r.at[p, place], dev(k, x, z, c))

    def p_from(src, place, p):
        return remote(src, fin.at[c, place, chunk(p)], p_s, p_r, here)

    def p_pass(place, p):
        return p_from(fin.at[c, place, chunk(p)], place, p)

    def p_keep(xs, p):
        slot = y * SIDE + xs
        return p_from(trans.at[slot, chunk(p)], slot, p)

    def goes_up(f, p):
        return f < far if p < EARLY else f < far - 1

    def goes_down(f, p):
        return f < far - 1 if p < EARLY else f < far

    def hand_over(k, xs, p):
        @pl.when(k != y)
        def _():
            y_move(k, xs, p, y * SIDE + xs).start()

        @pl.when(k == y)
        def _():
            slot = k * SIDE + xs
            p_keep(xs, p).start()
            fin[c, slot, p * cut:(p + 1) * cut] = trans[slot, p * cut:(p + 1) * cut]

    @pl.when(~origin)
    def _():
        for p in range(PARTS):
            x_copy(x, p).start()

    e = lax.rem(z - x + planes, SIDE)
    lower = jnp.where(e == 0, SIDE, e)
    upper = SIDE - e

    def ring(i, carry):
        ib = i - lower
        ia = i - upper
        db = lower + SIDE * (ib // SIDE)
        da = upper + SIDE * (ia // SIDE)
        kb = around(z - db, planes) // SIDE
        ka = around(z + da, planes) // SIDE
        xb = lax.rem(ib + SIDE, SIDE)
        xa = lax.rem(ia + SIDE, SIDE)
        for p in range(PARTS):
            @pl.when(origin & (i < SIDE))
            def _():
                xs = lax.rem(x + i, SIDE)
                slot = kq * SIDE + xs

                @pl.when(i > 0)
                def _():
                    x_copy(xs, p).wait_recv()
                up_move(slot, p).start()
                down_move(slot, p).start()
                hand_over(kq, xs, p)

            @pl.when((ib >= 0) & (ib < 2 * SIDE) & ((db < far) | (p < EARLY)))
            def _():
                slot = kb * SIDE + lax.rem(x + xb, SIDE)
                up_move(slot, p).wait_recv()

                @pl.when(goes_up(db, p))
                def _():
                    up_move(slot, p).start()
                hand_over(kb, lax.rem(x + xb, SIDE), p)

            @pl.when((ia >= 0) & (ia < 2 * SIDE) & ((da < far) | (p >= EARLY)))
            def _():
                slot = ka * SIDE + lax.rem(x + xa, SIDE)
                down_move(slot, p).wait_recv()

                @pl.when(goes_down(da, p))
                def _():
                    down_move(slot, p).start()
                hand_over(ka, lax.rem(x + xa, SIDE), p)
        return carry

    lax.fori_loop(0, 3 * SIDE, ring, 0)

    def pass_on(xs, carry):
        for p in range(PARTS):
            for o in range(1, SIDE):
                place = around(y + o, SIDE) * SIDE + xs
                y_move(y, xs, p, place).wait_recv()
                p_pass(place, p).start()
        return carry

    lax.fori_loop(0, SIDE, pass_on, 0)

    pltpu.make_async_copy(trans, trans, p_r).wait()
    pltpu.make_async_copy(trans, trans, p_s).wait()
    kept = trans.at[pl.ds(0, spots - SIDE)]
    pltpu.make_async_copy(kept, kept, y_s).wait()

    def swept(sem, short, cuts):
        whole = trans.at[pl.ds(0, 2 * SIDE)]
        less = trans.at[pl.ds(0, SIDE * (PARTS + cuts) // 2), pl.ds(0, 2 * cut)]

        @pl.when(short)
        def _():
            pltpu.make_async_copy(less, less, sem).wait()

        @pl.when(~short)
        def _():
            pltpu.make_async_copy(whole, whole, sem).wait()

    swept(up_s, e == SIDE - 1, EARLY)
    swept(down_s, e == 1, PARTS - EARLY)

    @pl.when(~origin)
    def _():
        pltpu.make_async_copy(own, own, x_s).wait()

    pltpu.make_async_copy(tokens.at[1], tokens.at[1], tok_s).wait()
    arrived(z_s, planes - 1, rcut + pcut, lcut)
    arrived(a_s, planes - 1, rcut, lcut * (SIDE - 1))
    arrived(b_s, planes - 1, rcut * (SIDE - 1), lat)
    arrived(t_s, planes - 1, pcut, rows * (SIDE - 1))


def read_kernel(steps, x_ref, up_ref, q_ref, plain_ref, value_ref, rot_ref, read_ref, held, scores):
    i = pl.program_id(0)
    part = i // steps
    step = lax.rem(i, steps)
    spots, block, lat = x_ref.shape[1:]
    kw = plain_ref.shape[2]
    span = rot_ref.shape[2] // (spots // steps)
    rope = rot_ref.shape[1]
    fold = block - span
    count = spots // steps
    chosen = jnp.where(part == 0, q_ref[:1].astype(F32), q_ref[1:].astype(F32)).astype(BF16)
    up = up_ref[...]
    contract = (((1,), (1,)), ((), ()))
    for n in range(count):
        spot = step * count + n
        both = jnp.dot(x_ref[part, spot, :span], up, preferred_element_type=F32)
        keys = both[:, :kw].astype(BF16)
        values = both[:, kw:].astype(BF16)
        plain_ref[0, n * span:(n + 1) * span] = keys
        value_ref[0, n * span:(n + 1) * span] = values
        held[pl.ds(pl.multiple_of(spot * span, span), span)] = values
        wide = x_ref[part, spot, span:]
        rotated = jnp.concatenate([wide[:, g * span:(g + 1) * span] for g in range(rope // fold)], axis=0)
        rot_ref[0, :, n * span:(n + 1) * span] = rotated
        score = lax.dot_general(chosen[:, :kw], keys, contract, preferred_element_type=F32)
        score = score + jnp.dot(chosen[:, kw:], rotated, preferred_element_type=F32)
        scores[pl.ds(spot, 1)] = score * (1.0 / (kw + rope) ** 0.5)

    @pl.when(step == steps - 1)
    def _():
        full = scores[...]
        weights = jnp.exp(full - jnp.max(full, keepdims=True))
        total = jnp.sum(weights, keepdims=True)
        rounded = weights.astype(BF16)
        mixed = jnp.zeros((1, value_ref.shape[2]), F32)
        for n in range(spots):
            mixed += jnp.dot(rounded[n:n + 1], held[n * span:(n + 1) * span], preferred_element_type=F32)
        mixed = mixed / total
        row = lax.broadcasted_iota(jnp.int32, read_ref.shape, 0)
        kept = jnp.where(row == part, mixed, read_ref[...].astype(F32))
        read_ref[...] = jnp.where((part > 0) | (row == 0), kept, 0.0).astype(BF16)


def body(planes, spots, tokens, latent_down, rope_weight, norm_scale, key_up, value_up, query):
    span = tokens.shape[1]
    rows, lat = latent_down.shape
    rope = rope_weight.shape[1]
    heads, kw = key_up.shape[1:]
    vw = value_up.shape[2]
    assert heads == 1
    length = spots * span
    block = span + rope * span // lat
    cosine, sine = turn_tables(np.arange(length + 1), rope)
    vmem = pl.BlockSpec(memory_space=pltpu.VMEM)
    hbm = pl.BlockSpec(memory_space=pl.ANY)
    dma = pltpu.SemaphoreType.DMA
    one = pltpu.SemaphoreType.DMA
    x_all, up, asked = pl.pallas_call(
        functools.partial(move_kernel, planes, spots),
        out_shape=(pltpu.VMEM((CORES, spots, block, lat), BF16),
                   pltpu.VMEM((lat, kw + vw), BF16),
                   pltpu.VMEM((CORES, kw + rope), BF16)),
        in_specs=[hbm] * 11,
        out_specs=(vmem, vmem, vmem),
        scratch_shapes=[
            pltpu.VMEM((CORES, planes, span, rows), BF16),
            pltpu.VMEM((planes, rows, lat), BF16),
            pltpu.VMEM((planes, rope, rows), BF16),
            pltpu.VMEM((CORES * span, lat), F32),
            pltpu.VMEM((rope, CORES * span), F32),
            pltpu.VMEM((span, lat), F32),
            pltpu.VMEM((rope, span), F32),
            pltpu.VMEM((block, lat), BF16),
            pltpu.VMEM((spots, block, lat), BF16),
            pltpu.VMEM((rope, span), F32),
            pltpu.VMEM((rope, span), F32),
            pltpu.VMEM((1, lat), F32),
            pltpu.VMEM((CORES, kw + rope), BF16),
            pltpu.VMEM((1, rope), F32),
            pltpu.VMEM((1, rope), F32),
            one, one, one, dma((10,)),
            one, dma((planes,)), one, dma((planes,)),
            one, dma((planes,)), one, dma((planes,)),
            dma((2,)), dma((2,)),
            one, dma((PARTS, SIDE)), one, one, dma((PARTS, spots)),
            one, dma((PARTS, spots)), one, one,
        ],
        compiler_params=pltpu.CompilerParams(collective_id=0, has_side_effects=True, vmem_limit_bytes=GRANT),
    )(tokens, latent_down, rope_weight.T, norm_scale.reshape(1, lat),
      jnp.asarray(np.ascontiguousarray(cosine[:length].T)), jnp.asarray(np.ascontiguousarray(sine[:length].T)),
      key_up.reshape(lat, kw), value_up.reshape(lat, vw), query.reshape(CORES, kw + rope),
      jnp.asarray(cosine[length:]), jnp.asarray(sine[length:]))

    def whole(shape):
        return pl.BlockSpec(shape, lambda i: (0,) * len(shape))

    wide = length // STEPS
    plain, value, rot, read = pl.pallas_call(
        functools.partial(read_kernel, STEPS),
        grid=(CORES * STEPS,),
        out_shape=(jax.ShapeDtypeStruct((CORES, length, kw), BF16),
                   jax.ShapeDtypeStruct((CORES, length, vw), BF16),
                   jax.ShapeDtypeStruct((CORES, rope, length), BF16),
                   jax.ShapeDtypeStruct((CORES, vw), BF16)),
        in_specs=[vmem, vmem, vmem],
        out_specs=(pl.BlockSpec((1, wide, kw), lambda i: (i // STEPS, i % STEPS, 0)),
                   pl.BlockSpec((1, wide, vw), lambda i: (i // STEPS, i % STEPS, 0)),
                   pl.BlockSpec((1, rope, wide), lambda i: (i // STEPS, 0, i % STEPS)), whole((CORES, vw))),
        scratch_shapes=[pltpu.VMEM((length, vw), BF16), pltpu.VMEM((spots, span), F32)],
        compiler_params=pltpu.CompilerParams(vmem_limit_bytes=READ_GRANT),
    )(x_all, up, asked)
    return (plain.reshape(CORES, length, heads, kw), value.reshape(CORES, length, heads, vw), jnp.swapaxes(rot, 1, 2),
            read.reshape(CORES, heads, vw))


def solution(mesh):
    planes = mesh.shape["tp"] // CORES
    spots = mesh.shape["sp"]
    assert planes == spots == SIDE * SIDE
    in_specs = (
        P("tp", "sp", None),
        P("tp", None),
        P("tp", None),
        P(),
        P(None, "tp", None),
        P(None, "tp", None),
        P("sp", "tp", None),
    )
    out_specs = (
        P("sp", None, "tp", None),
        P("sp", None, "tp", None),
        P("sp", None, None),
        P("sp", "tp", None),
    )
    return jax.shard_map(functools.partial(body, planes, spots), mesh=mesh, in_specs=in_specs,
                         out_specs=out_specs, check_vma=False)
```

time: 116 us -> 108 us (0.931)
  Pallas kernels: 115 us -> 107 us
    pallas_call x1, Pallas kernels: 109 us -> 98.9 us  [body(): pl.pallas_call(functools.partial(move_kernel, planes, spots), out_shape=(...]
    pallas_call x1, Pallas kernels: 5.73 us -> 7.85 us  [body(): pl.pallas_call(functools.partial(read_kernel, STEPS), grid=(CORES * STEPS...]
where the time goes in v2:
time: 108 us; the launch traced here: 107 us
  Pallas kernels  107 us (99%)
    pallas_call x1, Pallas kernels, body(): pl.pallas_call(functools.partial(move_kernel, planes, spots), out_shape=(...  98.9 us
    pallas_call x1, Pallas kernels, body(): pl.pallas_call(functools.partial(read_kernel, STEPS), grid=(CORES * STEPS...  7.85 us

profile of v2, /device:TPU:51, one launch (start us, length us, event | category | flops | bytes accessed | tf_op | source)
XLA Modules:
  0.0 107.4 jit_solution(2946839174443244090)
XLA Ops:
  0.6 98.9 %shard_map.138 = (bf16[2,16,144,512]{3,2,1,0:T(8,128)(2,1)S(1)}, bf16[512,256]{1,0:T(8,128)(2,1)S(1)}, bf16[2,192]{1,0:T(2,128)(2,1)S(1)}) custom-call(bf16[1,128,4096]{2,1,0:T(8,128)(2,1)} %tok.1, bf16[128,512]{1,0:T(8,128)(2,1)} %wl.1, bf16[64,128]{1,0:T(8,128)(2,1)} %bitcast.15, f32[1,512]{1,0:T(1,128)} %bitcast.16, f32[64,2048]{1,0:T(8,128)} %constant.8.clone.cos_hbm, ...), custom_call_target="tpu_custom_call" | custom-call | tf_op jit(solution)/shard_map/pallas_call | solution.py:447
  99.5 7.8 %shard_map.139 = (bf16[2,2048,128]{2,1,0:T(8,128)(2,1)}, bf16[2,2048,128]{2,1,0:T(8,128)(2,1)}, bf16[2,64,2048]{2,1,0:T(8,128)(2,1)}, bf16[2,128]{1,0:T(2,128)(2,1)}) custom-call(bf16[2,16,144,512]{3,2,1,0:T(8,128)(2,1)S(1)} %get-tuple-element.11.x_ref, bf16[512,256]{1,0:T(8,128)(2,1)S(1)} %get-tuple-element.12.up_ref, ...), custom_call_target="tpu_custom_call" | custom-call | tf_op jit(solution)/shard_map/pallas_call | solution.py:487

commit v3 on v2

--- a/solution.py
+++ b/solution.py
@@ -12,7 +12,9 @@
 SIDE = 4
 PARTS = 3
 EARLY = 2
-STEPS = 4
+NEAR = 1
+LAG = 4
+HUB = 4
 GRANT = 61_900_000
 READ_GRANT = 40_000_000
 BF16 = jnp.bfloat16
@@ -123,10 +125,11 @@
     def r_piece(u, i):
         return wrope.at[u, pl.ds(pl.multiple_of(i * pcut, 16), pcut)]
 
-    def z_copy(u, zi, i):
+    def z_copy(u, zi, by_row, near):
         where = dev(y, x, zi, c)
-        return [remote(w_piece(u), w_piece(u), z_s, z_r.at[u], where),
-                remote(r_piece(u, i), r_piece(u, i), z_s, z_r.at[u], where)]
+        part = (w_row(u) if by_row else w_col(u)) if near else w_piece(u)
+        turned = r_piece(u, y if by_row else x)
+        return [remote(part, part, z_s, z_r.at[u], where), remote(turned, turned, z_s, z_r.at[u], where)]
 
     def a_copy(u, o, by_row):
         where = dev(y, around(x + o, SIDE), z, c) if by_row else dev(around(y + o, SIDE), x, z, c)
@@ -149,15 +152,14 @@
     def above(d):
         return around(z + d, planes)
 
-    def z_send(d, carry):
-        each(z_copy(z, above(d), y), "start")
-
-        @pl.when(d < far)
-        def _():
-            each(z_copy(z, below(d), x), "start")
-        return carry
-
-    lax.fori_loop(1, far + 1, z_send, 0)
+    for d in range(1, NEAR + 1):
+        each(z_copy(z, above(d), True, True), "start")
+        each(z_copy(z, below(d), False, True), "start")
+
+    for d in range(NEAR + 1, HUB + 1):
+        each(z_copy(z, above(d), True, False), "start")
+        each(z_copy(z, below(d), False, False), "start")
+
     for u in range(planes):
         part_tok(u).start()
     each(tables, "start")
@@ -176,13 +178,21 @@
         acc[...] = a
         acct[...] = b
 
+    def spread(u, by_row):
+        for o in range(1, SIDE):
+            a_copy(u, o, by_row).start()
+
     def first(u, by_row):
         arrived(z_r.at[u], 1, rcut + pcut, lcut)
-        for o in range(1, SIDE):
-            a_copy(u, o, by_row).start()
+        spread(u, by_row)
 
     def second(u, by_row):
         arrived(a_r.at[u], 1, rcut, lcut * (SIDE - 1))
+        for o in range(1, SIDE):
+            each(b_copy(u, o, by_row), "start")
+
+    def nearby(u, by_row):
+        arrived(z_r.at[u], 1, rcut + pcut, lcut * (SIDE - 1))
         for o in range(1, SIDE):
             each(b_copy(u, o, by_row), "start")
 
@@ -193,27 +203,43 @@
         acc[...] += a
         acct[...] += b
 
-    def both(d, what):
-        @pl.when((d >= 1) & (d <= far))
+    def both(d, low, what):
+        @pl.when((d >= low) & (d <= far))
         def _():
             what(below(d), True)
 
-        @pl.when((d >= 1) & (d < far))
+        @pl.when((d >= low) & (d < far))
         def _():
             what(above(d), False)
 
+    for d in range(1, NEAR + 1):
+        nearby(below(d), True)
+        nearby(above(d), False)
+
+    arrived(z_r.at[below(HUB)], 1, rcut + pcut, lcut)
+    for d in range(1, far - HUB + 1):
+        each(z_copy(below(HUB), above(d), True, False), "start")
+    arrived(z_r.at[above(HUB)], 1, rcut + pcut, lcut)
+    for d in range(1, far - HUB):
+        each(z_copy(above(HUB), below(d), False, False), "start")
+    spread(below(HUB), True)
+    spread(above(HUB), False)
+    for d in range(NEAR + 1, HUB):
+        first(below(d), True)
+        first(above(d), False)
+
     def step(i, carry):
-        both(i, first)
-        both(i - 2, second)
-
-        @pl.when(i == 3)
+        both(i + HUB - NEAR, HUB + 1, first)
+
+        @pl.when(i == NEAR + 1)
         def _():
             own_block()
 
-        both(i - 4, third)
+        both(i, NEAR + 1, second)
+        both(i - LAG, 1, third)
         return carry
 
-    lax.fori_loop(1, far + 5, step, 0)
+    lax.fori_loop(NEAR + 1, far + LAG + 1, step, 0)
 
     swaps = [remote(acc.at[pl.ds(span, span)], other, acc_s.at[0], acc_r.at[0], here),
              remote(acct.at[:, pl.ds(span, span)], othert, acc_s.at[1], acc_r.at[1], here)]
@@ -381,53 +407,40 @@
         pltpu.make_async_copy(own, own, x_s).wait()
 
     pltpu.make_async_copy(tokens.at[1], tokens.at[1], tok_s).wait()
-    arrived(z_s, planes - 1, rcut + pcut, lcut)
-    arrived(a_s, planes - 1, rcut, lcut * (SIDE - 1))
+    arrived(z_s, planes - 1 - 2 * NEAR, rcut + pcut, lcut)
+    arrived(z_s, 2 * NEAR, rcut + pcut, lcut * (SIDE - 1))
+    arrived(a_s, planes - 1 - 2 * NEAR, rcut, lcut * (SIDE - 1))
     arrived(b_s, planes - 1, rcut * (SIDE - 1), lat)
     arrived(t_s, planes - 1, pcut, rows * (SIDE - 1))
 
 
-def read_kernel(steps, x_ref, up_ref, q_ref, plain_ref, value_ref, rot_ref, read_ref, held, scores):
-    i = pl.program_id(0)
-    part = i // steps
-    step = lax.rem(i, steps)
+def read_kernel(x_ref, up_ref, q_ref, plain_ref, value_ref, rot_ref, read_ref):
+    part = pl.program_id(0)
     spots, block, lat = x_ref.shape[1:]
-    kw = plain_ref.shape[2]
-    span = rot_ref.shape[2] // (spots // steps)
+    length, kw = plain_ref.shape[1:]
     rope = rot_ref.shape[1]
+    span = length // spots
     fold = block - span
-    count = spots // steps
+    wide = x_ref[part, :, span:]
+    for g in range(rope // fold):
+        for n in range(spots):
+            rot_ref[0, g * fold:(g + 1) * fold, n * span:(n + 1) * span] = wide[n, :, g * span:(g + 1) * span]
+    both = jnp.dot(x_ref[part, :, :span].reshape(length, lat), up_ref[...], preferred_element_type=F32).astype(BF16)
+    keys = both[:, :kw]
+    values = both[:, kw:]
+    plain_ref[0] = keys
+    value_ref[0] = values
     chosen = jnp.where(part == 0, q_ref[:1].astype(F32), q_ref[1:].astype(F32)).astype(BF16)
-    up = up_ref[...]
     contract = (((1,), (1,)), ((), ()))
-    for n in range(count):
-        spot = step * count + n
-        both = jnp.dot(x_ref[part, spot, :span], up, preferred_element_type=F32)
-        keys = both[:, :kw].astype(BF16)
-        values = both[:, kw:].astype(BF16)
-        plain_ref[0, n * span:(n + 1) * span] = keys
-        value_ref[0, n * span:(n + 1) * span] = values
-        held[pl.ds(pl.multiple_of(spot * span, span), span)] = values
-        wide = x_ref[part, spot, span:]
-        rotated = jnp.concatenate([wide[:, g * span:(g + 1) * span] for g in range(rope // fold)], axis=0)
-        rot_ref[0, :, n * span:(n + 1) * span] = rotated
-        score = lax.dot_general(chosen[:, :kw], keys, contract, preferred_element_type=F32)
-        score = score + jnp.dot(chosen[:, kw:], rotated, preferred_element_type=F32)
-        scores[pl.ds(spot, 1)] = score * (1.0 / (kw + rope) ** 0.5)
-
-    @pl.when(step == steps - 1)
-    def _():
-        full = scores[...]
-        weights = jnp.exp(full - jnp.max(full, keepdims=True))
-        total = jnp.sum(weights, keepdims=True)
-        rounded = weights.astype(BF16)
-        mixed = jnp.zeros((1, value_ref.shape[2]), F32)
-        for n in range(spots):
-            mixed += jnp.dot(rounded[n:n + 1], held[n * span:(n + 1) * span], preferred_element_type=F32)
-        mixed = mixed / total
-        row = lax.broadcasted_iota(jnp.int32, read_ref.shape, 0)
-        kept = jnp.where(row == part, mixed, read_ref[...].astype(F32))
-        read_ref[...] = jnp.where((part > 0) | (row == 0), kept, 0.0).astype(BF16)
+    scores = lax.dot_general(chosen[:, :kw], keys, contract, preferred_element_type=F32)
+    scores = scores + jnp.dot(chosen[:, kw:], rot_ref[0], preferred_element_type=F32)
+    scores = scores * (1.0 / (kw + rope) ** 0.5)
+    weights = jnp.exp(scores - jnp.max(scores, axis=-1, keepdims=True))
+    total = jnp.sum(weights, axis=-1, keepdims=True)
+    mixed = jnp.dot(weights.astype(BF16), values, preferred_element_type=F32) / total
+    row = lax.broadcasted_iota(jnp.int32, read_ref.shape, 0)
+    kept = jnp.where(row == part, mixed, read_ref[...].astype(F32))
+    read_ref[...] = jnp.where((part > 0) | (row == 0), kept, 0.0).astype(BF16)
 
 
 def body(planes, spots, tokens, latent_down, rope_weight, norm_scale, key_up, value_up, query):
@@ -483,19 +496,18 @@
     def whole(shape):
         return pl.BlockSpec(shape, lambda i: (0,) * len(shape))
 
-    wide = length // STEPS
+    def per(shape):
+        return pl.BlockSpec((1,) + shape, lambda i: (i,) + (0,) * len(shape))
+
     plain, value, rot, read = pl.pallas_call(
-        functools.partial(read_kernel, STEPS),
-        grid=(CORES * STEPS,),
+        read_kernel,
+        grid=(CORES,),
         out_shape=(jax.ShapeDtypeStruct((CORES, length, kw), BF16),
                    jax.ShapeDtypeStruct((CORES, length, vw), BF16),
                    jax.ShapeDtypeStruct((CORES, rope, length), BF16),
                    jax.ShapeDtypeStruct((CORES, vw), BF16)),
         in_specs=[vmem, vmem, vmem],
-        out_specs=(pl.BlockSpec((1, wide, kw), lambda i: (i // STEPS, i % STEPS, 0)),
-                   pl.BlockSpec((1, wide, vw), lambda i: (i // STEPS, i % STEPS, 0)),
-                   pl.BlockSpec((1, rope, wide), lambda i: (i // STEPS, 0, i % STEPS)), whole((CORES, vw))),
-        scratch_shapes=[pltpu.VMEM((length, vw), BF16), pltpu.VMEM((spots, span), F32)],
+        out_specs=(per((length, kw)), per((length, vw)), per((rope, length)), whole((CORES, vw))),
         compiler_params=pltpu.CompilerParams(vmem_limit_bytes=READ_GRANT),
     )(x_all, up, asked)
     return (plain.reshape(CORES, length, heads, kw), value.reshape(CORES, length, heads, vw), jnp.swapaxes(rot, 1, 2),

time: 108 us -> 102 us (0.944)
  Pallas kernels: 107 us -> 101 us
    pallas_call x1, Pallas kernels: 7.85 us -> 3.45 us  [body(): pl.pallas_call(read_kernel, grid=(CORES,), out_shape=(jax.ShapeDtypeStruc...]
where the time goes in v3:
time: 102 us
  Pallas kernels  101 us (99%)
    pallas_call x1, Pallas kernels, body(): pl.pallas_call(functools.partial(move_kernel, planes, spots), out_shape=(...  97.8 us
    pallas_call x1, Pallas kernels, body(): pl.pallas_call(read_kernel, grid=(CORES,), out_shape=(jax.ShapeDtypeStruc...  3.45 us

profile of v3, /device:TPU:51, one launch (start us, length us, event | category | flops | bytes accessed | tf_op | source)
XLA Modules:
  0.0 101.9 jit_solution(16942408324891602940)
XLA Ops:
  0.6 97.8 %shard_map.138 = (bf16[2,16,144,512]{3,2,1,0:T(8,128)(2,1)S(1)}, bf16[512,256]{1,0:T(8,128)(2,1)S(1)}, bf16[2,192]{1,0:T(2,128)(2,1)S(1)}) custom-call(bf16[1,128,4096]{2,1,0:T(8,128)(2,1)} %tok.1, bf16[128,512]{1,0:T(8,128)(2,1)} %wl.1, bf16[64,128]{1,0:T(8,128)(2,1)} %bitcast.15, f32[1,512]{1,0:T(1,128)} %bitcast.16, f32[64,2048]{1,0:T(8,128)} %constant.8.clone.cos_hbm, ...), custom_call_target="tpu_custom_call" | custom-call | tf_op jit(solution)/shard_map/pallas_call | solution.py:460
  98.5 3.4 %shard_map.139 = (bf16[2,2048,128]{2,1,0:T(8,128)(2,1)}, bf16[2,2048,128]{2,1,0:T(8,128)(2,1)}, bf16[2,64,2048]{2,1,0:T(8,128)(2,1)}, bf16[2,128]{1,0:T(2,128)(2,1)}) custom-call(bf16[2,16,144,512]{3,2,1,0:T(8,128)(2,1)S(1)} %get-tuple-element.11.x_ref, bf16[512,256]{1,0:T(8,128)(2,1)S(1)} %get-tuple-element.12.up_ref, ...), custom_call_target="tpu_custom_call" | custom-call | tf_op jit(solution)/shard_map/pallas_call | solution.py:502

commit v4 on v3

--- a/solution.py
+++ b/solution.py
@@ -13,7 +13,7 @@
 PARTS = 3
 EARLY = 2
 NEAR = 1
-LAG = 4
+LAG = 5
 HUB = 4
 GRANT = 61_900_000
 READ_GRANT = 40_000_000
@@ -38,7 +38,7 @@
 
 def move_kernel(planes, spots, tok, wl, wr, scale_hbm, cos_hbm, sin_hbm, kup, vup, q_hbm, qcos_hbm, qsin_hbm, fin, up, ask,
                 tokens, wlat, wrope, acc, acct, other, othert, own, trans, cos_ref, sin_ref, scale, query, qcos, qsin,
-                tok_s, tok_r, tok_o, own_s, z_s, z_r, a_s, a_r, b_s, b_r, t_s, t_r,
+                tok_s, tok_r, tok_o, own_s, z_s, z_r, a_s, a_r, b_s, b_r,
                 acc_s, acc_r, x_s, x_r, up_s, down_s, in_r, y_s, y_r, p_s, p_r):
     s = lax.axis_index("sp")
     t = lax.axis_index("tp")
@@ -140,7 +140,7 @@
         part = w_row(u) if by_row else w_col(u)
         turned = r_piece(u, y if by_row else x)
         return [remote(part, part, b_s, b_r.at[u], where),
-                remote(turned, turned, t_s, t_r.at[u], where)]
+                remote(turned, turned, b_s, b_r.at[u], where)]
 
     def arrived(sem, count, deep, wide):
         part = wlat.at[pl.ds(0, count), pl.ds(0, deep), pl.ds(0, wide)]
@@ -152,13 +152,9 @@
     def above(d):
         return around(z + d, planes)
 
-    for d in range(1, NEAR + 1):
-        each(z_copy(z, above(d), True, True), "start")
-        each(z_copy(z, below(d), False, True), "start")
-
-    for d in range(NEAR + 1, HUB + 1):
-        each(z_copy(z, above(d), True, False), "start")
-        each(z_copy(z, below(d), False, False), "start")
+    for d in range(HUB, 0, -1):
+        each(z_copy(z, above(d), True, d <= NEAR), "start")
+        each(z_copy(z, below(d), False, d <= NEAR), "start")
 
     for u in range(planes):
         part_tok(u).start()
@@ -197,8 +193,7 @@
             each(b_copy(u, o, by_row), "start")
 
     def third(u, by_row):
-        arrived(b_r.at[u], 1, rcut * (SIDE - 1), lat)
-        arrived(t_r.at[u], 1, pcut, rows * (SIDE - 1))
+        arrived(b_r.at[u], (SIDE - 1) * (SIDE - 1), rcut + pcut, lcut)
         a, b = block_dot(u)
         acc[...] += a
         acct[...] += b
@@ -289,13 +284,10 @@
         return z_move(slot, p, around(z - 1, planes), down_s)
 
     def y_move(k, xs, p, place):
-        return remote(trans.at[k * SIDE + xs, chunk(p)], fin.at[c, place, chunk(p)], y_s, y_r.at[p, place], dev(k, x, z, c))
+        return remote(trans.at[k * SIDE + xs, chunk(p)], fin.at[c, place, chunk(p)], y_s, y_r.at[place], dev(k, x, z, c))
 
     def p_from(src, place, p):
         return remote(src, fin.at[c, place, chunk(p)], p_s, p_r, here)
-
-    def p_pass(place, p):
-        return p_from(fin.at[c, place, chunk(p)], place, p)
 
     def p_keep(xs, p):
         slot = y * SIDE + xs
@@ -326,6 +318,9 @@
     e = lax.rem(z - x + planes, SIDE)
     lower = jnp.where(e == 0, SIDE, e)
     upper = SIDE - e
+
+    def across(o):
+        return jnp.where(o == 2, 3, jnp.where(o == 3, 2, o))
 
     def ring(i, carry):
         ib = i - lower
@@ -339,7 +334,7 @@
         for p in range(PARTS):
             @pl.when(origin & (i < SIDE))
             def _():
-                xs = lax.rem(x + i, SIDE)
+                xs = lax.rem(x + across(i), SIDE)
                 slot = kq * SIDE + xs
 
                 @pl.when(i > 0)
@@ -351,33 +346,33 @@
 
             @pl.when((ib >= 0) & (ib < 2 * SIDE) & ((db < far) | (p < EARLY)))
             def _():
-                slot = kb * SIDE + lax.rem(x + xb, SIDE)
+                slot = kb * SIDE + lax.rem(x + across(xb), SIDE)
                 up_move(slot, p).wait_recv()
 
                 @pl.when(goes_up(db, p))
                 def _():
                     up_move(slot, p).start()
-                hand_over(kb, lax.rem(x + xb, SIDE), p)
+                hand_over(kb, lax.rem(x + across(xb), SIDE), p)
 
             @pl.when((ia >= 0) & (ia < 2 * SIDE) & ((da < far) | (p >= EARLY)))
             def _():
-                slot = ka * SIDE + lax.rem(x + xa, SIDE)
+                slot = ka * SIDE + lax.rem(x + across(xa), SIDE)
                 down_move(slot, p).wait_recv()
 
                 @pl.when(goes_down(da, p))
                 def _():
                     down_move(slot, p).start()
-                hand_over(ka, lax.rem(x + xa, SIDE), p)
+                hand_over(ka, lax.rem(x + across(xa), SIDE), p)
         return carry
 
     lax.fori_loop(0, 3 * SIDE, ring, 0)
 
     def pass_on(xs, carry):
-        for p in range(PARTS):
-            for o in range(1, SIDE):
-                place = around(y + o, SIDE) * SIDE + xs
-                y_move(y, xs, p, place).wait_recv()
-                p_pass(place, p).start()
+        for o in range(1, SIDE):
+            place = around(y + o, SIDE) * SIDE + xs
+            whole = fin.at[c, place]
+            pltpu.make_async_copy(whole, whole, y_r.at[place]).wait()
+            remote(whole, whole, p_s, p_r, here).start()
         return carry
 
     lax.fori_loop(0, SIDE, pass_on, 0)
@@ -411,7 +406,7 @@
     arrived(z_s, 2 * NEAR, rcut + pcut, lcut * (SIDE - 1))
     arrived(a_s, planes - 1 - 2 * NEAR, rcut, lcut * (SIDE - 1))
     arrived(b_s, planes - 1, rcut * (SIDE - 1), lat)
-    arrived(t_s, planes - 1, pcut, rows * (SIDE - 1))
+    arrived(b_s, planes - 1, pcut, rows * (SIDE - 1))
 
 
 def read_kernel(x_ref, up_ref, q_ref, plain_ref, value_ref, rot_ref, read_ref):
@@ -482,10 +477,10 @@
             pltpu.VMEM((1, rope), F32),
             one, one, one, dma((10,)),
             one, dma((planes,)), one, dma((planes,)),
-            one, dma((planes,)), one, dma((planes,)),
+            one, dma((planes,)),
             dma((2,)), dma((2,)),
             one, dma((PARTS, SIDE)), one, one, dma((PARTS, spots)),
-            one, dma((PARTS, spots)), one, one,
+            one, dma((spots,)), one, one,
         ],
         compiler_params=pltpu.CompilerParams(collective_id=0, has_side_effects=True, vmem_limit_bytes=GRANT),
     )(tokens, latent_down, rope_weight.T, norm_scale.reshape(1, lat),

time: 102 us -> 101 us (level)
  the two profiles are of different devices: /device:TPU:51 before, /device:TPU:15 now
where the time goes in v4:
time: 101 us
  Pallas kernels  100 us (99%)
    pallas_call x1, Pallas kernels, body(): pl.pallas_call(functools.partial(move_kernel, planes, spots), out_shape=(...  96.8 us
    pallas_call x1, Pallas kernels, body(): pl.pallas_call(read_kernel, grid=(CORES,), out_shape=(jax.ShapeDtypeStruc...  3.45 us

profile of v4, /device:TPU:15, one launch (start us, length us, event | category | flops | bytes accessed | tf_op | source)
XLA Modules:
  0.0 100.9 jit_solution(13872165738480483580)
XLA Ops:
  0.6 96.8 %shard_map.138 = (bf16[2,16,144,512]{3,2,1,0:T(8,128)(2,1)S(1)}, bf16[512,256]{1,0:T(8,128)(2,1)S(1)}, bf16[2,192]{1,0:T(2,128)(2,1)S(1)}) custom-call(bf16[1,128,4096]{2,1,0:T(8,128)(2,1)} %tok.1, bf16[128,512]{1,0:T(8,128)(2,1)} %wl.1, bf16[64,128]{1,0:T(8,128)(2,1)} %bitcast.15, f32[1,512]{1,0:T(1,128)} %bitcast.16, f32[64,2048]{1,0:T(8,128)} %constant.8.clone.cos_hbm, ...), custom_call_target="tpu_custom_call" | custom-call | tf_op jit(solution)/shard_map/pallas_call | solution.py:455
  97.4 3.4 %shard_map.139 = (bf16[2,2048,128]{2,1,0:T(8,128)(2,1)}, bf16[2,2048,128]{2,1,0:T(8,128)(2,1)}, bf16[2,64,2048]{2,1,0:T(8,128)(2,1)}, bf16[2,128]{1,0:T(2,128)(2,1)}) custom-call(bf16[2,16,144,512]{3,2,1,0:T(8,128)(2,1)S(1)} %get-tuple-element.11.x_ref, bf16[512,256]{1,0:T(8,128)(2,1)S(1)} %get-tuple-element.12.up_ref, ...), custom_call_target="tpu_custom_call" | custom-call | tf_op jit(solution)/shard_map/pallas_call | solution.py:497
